TPU v7x, 128 devices: a whole 4x4x4 slice. The times are simulated.
128 devices in a mesh: rep: 2 (over z_hi), fs: 32 (over z_lo, y, x), tp: 2 (over core).
Axes of the slice: x: 4, y: 4, z: 4 (z_hi: 2, z_lo: 2; z = z_hi * 2 + z_lo), core: 2. Of those that a mesh axis runs over, the one named last changes fastest.
Arguments:
- stream_in: bfloat16 [64, 768, 2048], P(('rep', 'fs'), None, 'tp'), may hold values from -6 to 6
- mix_gain: float32 [2048], replicated, may hold values from 0.1 to 1.9
- lin_weight: bfloat16 [2048, 2048], P('fs', 'tp'), may hold values from -0.125 to 0.125
- branch_weight: bfloat16 [2048, 2048], P('fs', 'tp'), may hold values from -0.125 to 0.125
- lin_taps: float32 [4, 2048], P(None, 'tp'), may hold values from -3 to 3
- rate_blocks: bfloat16 [16, 128, 128], P('tp'), may hold values from -0.5 to 0.5
- admit_blocks: bfloat16 [16, 128, 128], P('tp'), may hold values from -0.5 to 0.5
- decay_logit: float32 [2048], P('tp'), may hold values from 3.5 to 9
- mix_out_gain: float32 [2048], P('tp'), may hold values from 0.1 to 1.9
- out_weight: bfloat16 [2048, 2048], P('tp', 'fs'), may hold values from -0.125 to 0.125
- ffn_gain: float32 [2048], replicated, may hold values from 0.1 to 1.9
- gate_weight: bfloat16 [2048, 2816], P('fs', 'tp'), may hold values from -0.125 to 0.125
- up_weight: bfloat16 [2048, 2816], P('fs', 'tp'), may hold values from -0.125 to 0.125
- gate_taps: float32 [3, 2816], P(None, 'tp'), may hold values from -3 to 3
- up_taps: float32 [3, 2816], P(None, 'tp'), may hold values from -3 to 3
- down_weight: bfloat16 [2816, 2048], P('tp', 'fs'), may hold values from -0.109375 to 0.109375
Outputs:
- stream_out: bfloat16 [64, 768, 2048], P(('rep', 'fs'), None, 'tp')
All inputs are finite; a program needn't handle non-finite values.
Results may differ from a plain program's by a relative error of at most 0.018.
Values may be sent and summed in bfloat16 or wider, within the bound.
A program may use at most 128 MiB of HBM per device.

v0:
```python
import jax
import jax.numpy as jnp
from jax import lax
from jax.sharding import PartitionSpec as P

EPS = 1e-06
GATE_SCALE = 8.0


def sent_to_all(value, axis):
    count = lax.axis_size(axis)
    return lax.all_to_all(
        jnp.broadcast_to(value[None], (count, *value.shape)), axis, 0, 0, tiled=True
    )


def in_order(tiles, dim):
    tiles = jnp.moveaxis(tiles, 0, dim)
    dims = tiles.shape
    return tiles.reshape(*dims[:dim], dims[dim] * dims[dim + 1], *dims[dim + 2 :])


def collect(value, axis, dim):
    tiles = sent_to_all(value, axis)
    return in_order(tiles, dim)


def side_by_side(arrays, axis, dim, along):
    widths = [a.shape[along] for a in arrays]
    both = jnp.concatenate(arrays, axis=along)
    whole = lax.all_gather(both, axis, axis=dim, tiled=True)
    return tuple(jnp.split(whole, [sum(widths[:k]) for k in range(1, len(widths))], axis=along))


def split_up(value, dim, count):
    before, after = (value.shape[:dim], value.shape[dim + 1 :])
    return jnp.moveaxis(value.reshape(*before, count, -1, *after), dim, 0)


def sent_and_summed(value, axis, dim):
    count = lax.axis_size(axis)
    tiles = lax.all_to_all(split_up(value, dim, count), axis, 0, 0, tiled=True)
    return jnp.sum(tiles.astype(jnp.float32), axis=0)


def norm_rows(values, scales):
    mean_sq = jnp.mean(values * values, axis=-1, keepdims=True)
    return values * lax.rsqrt(mean_sq + EPS) * scales


def causal_filter(values, kernel):
    kernel_len = kernel.shape[0]
    seq_len = values.shape[0]
    padded = jnp.pad(values, ((kernel_len - 1, 0), (0, 0)))
    summed = padded[0:seq_len] * kernel[0]
    for offset in range(1, kernel_len):
        summed = summed + padded[offset : offset + seq_len] * kernel[offset]
    return summed


def chain_combine(earlier, later):
    return (earlier[0] * later[0], later[0] * earlier[1] + later[1])


def pair_folder(source, pieces):
    return (
        jnp.dot(source, pieces[0], preferred_element_type=jnp.float32),
        jnp.dot(source, pieces[1], preferred_element_type=jnp.float32),
    )


def local(
    stream_in,
    mix_gain,
    lin_weight,
    branch_weight,
    lin_taps,
    rate_blocks,
    admit_blocks,
    decay_logit,
    mix_out_gain,
    out_weight,
    ffn_gain,
    gate_weight,
    up_weight,
    gate_taps,
    up_taps,
    down_weight,
):
    own_rows = stream_in[0]
    length = own_rows.shape[0]
    full_rows = collect(own_rows, "tp", 1)
    normed = norm_rows(full_rows.astype(jnp.float32), mix_gain).astype(jnp.bfloat16)
    linear, branch = pair_folder(normed, side_by_side((lin_weight, branch_weight), "fs", 0, 1))
    linear = linear.astype(jnp.bfloat16)
    branch = branch.astype(jnp.bfloat16)
    filtered = causal_filter(linear.astype(jnp.float32), lin_taps)
    block_count = rate_blocks.shape[0]
    block_width = rate_blocks.shape[1]
    blocks = filtered.astype(jnp.bfloat16).reshape(length, block_count, block_width)
    rate_gate = jax.nn.sigmoid(
        jnp.einsum("lbi,bij->lbj", blocks, rate_blocks, preferred_element_type=jnp.float32).reshape(
            length, -1
        )
    )
    admitted = jax.nn.sigmoid(
        jnp.einsum(
            "lbi,bij->lbj", blocks, admit_blocks, preferred_element_type=jnp.float32
        ).reshape(length, -1)
    )
    log_decay = -GATE_SCALE * rate_gate * jax.nn.softplus(-decay_logit)
    decay = jnp.exp(log_decay)
    driven = jnp.sqrt(-jnp.expm1(2.0 * log_decay)) * admitted * filtered
    _, states = lax.associative_scan(chain_combine, (decay, driven), axis=0)
    gated = (states * jax.nn.gelu(branch.astype(jnp.float32))).reshape(
        length, block_count, block_width
    )
    gated = gated * lax.rsqrt(jnp.mean(gated * gated, axis=-1, keepdims=True) + EPS)
    mixed = (gated.reshape(length, -1) * mix_out_gain).astype(jnp.bfloat16)
    mix_partial = jnp.dot(
        mixed,
        lax.all_gather(out_weight, "fs", axis=1, tiled=True),
        preferred_element_type=jnp.float32,
    )
    my_share = sent_and_summed(mix_partial.astype(jnp.bfloat16), "tp", 1)
    middle_own = (own_rows.astype(jnp.float32) + my_share).astype(jnp.bfloat16)
    middle_full = collect(middle_own, "tp", 1)
    normed2 = norm_rows(middle_full.astype(jnp.float32), ffn_gain).astype(jnp.bfloat16)
    gate_pre, up_pre = pair_folder(normed2, side_by_side((gate_weight, up_weight), "fs", 0, 1))
    gate_pre = gate_pre.astype(jnp.bfloat16)
    up_pre = up_pre.astype(jnp.bfloat16)
    gate_conv = causal_filter(gate_pre.astype(jnp.float32), gate_taps)
    up_conv = causal_filter(up_pre.astype(jnp.float32), up_taps)
    hidden = (jax.nn.silu(gate_conv) * up_conv).astype(jnp.bfloat16)
    down_partial = jnp.dot(
        hidden,
        lax.all_gather(down_weight, "fs", axis=1, tiled=True),
        preferred_element_type=jnp.float32,
    )
    down_share = sent_and_summed(down_partial.astype(jnp.bfloat16), "tp", 1)
    result = (middle_own.astype(jnp.float32) + down_share).astype(jnp.bfloat16)
    return result[None]


def solution(mesh):
    placed = (
        P(("rep", "fs"), None, "tp"),
        P(),
        P("fs", "tp"),
        P("fs", "tp"),
        P(None, "tp"),
        P("tp", None, None),
        P("tp", None, None),
        P("tp"),
        P("tp"),
        P("tp", "fs"),
        P(),
        P("fs", "tp"),
        P("fs", "tp"),
        P(None, "tp"),
        P(None, "tp"),
        P("tp", "fs"),
    )
    return jax.shard_map(
        local, mesh=mesh, in_specs=placed, out_specs=P(("rep", "fs"), None, "tp"), check_vma=False
    )
```

profile of v0, /device:TPU:1, one launch (start us, length us, event | category | flops | bytes accessed | tf_op | source)
XLA Modules:
  0.0 707.7 jit_solution(17645392529465928909)
XLA Ops:
  14.5 5.3 all-to-all-start
  20.4 2.6 all-to-all-done
  24.5 2.4 fusion.3
  26.9 131.2 %all-gather.5.cloned.1.call-done = bf16[2048,2048]{1,0:T(8,128)(2,1)} async-done(((bf16[64,2048]{1,0:T(8,128)(2,1)}), bf16[2048,2048]{1,0:T(8,128)(2,1)}) %all-gather.5.cloned.1.call-update) | async-done | bytes 8388624 | tf_op jit(solution)/shard_map/all_gather | solution.py:31
  158.1 6.7 fusion.38
  164.8 3.1 convert_bitcast_fusion
  169.0 2.3 copy.66
  171.3 2.5 add_divide_fusion
  173.8 2.4 copy.67
  176.2 7.6 %multiply_exponential_fusion = (f32[768,1024]{1,0:T(8,128)}, f32[768,1024]{1,0:T(8,128)S(1)}) fusion(f32[768,1024]{1,0:T(8,128)} %copy.66, f32[1024]{0:T(1024)S(1)} %fusion.62, f32[768,1024]{1,0:T(8,128)} %get-tuple-element.14, f32[768,1024]{1,0:T(8,128)} %copy.67), kind=kLoop, calls=%fused_computation.51 | loop fusion | flops 3932160 | bytes 15732736 | tf_op jit(solution)/shard_map/exp | solution.py:112
  183.8 4.2 slice.277
  188.0 4.2 slice.278
  192.1 7.6 %slice.276 = f32[384,1024]{1,0:T(8,128)} slice(f32[768,1024]{1,0:T(8,128)} %get-tuple-element.15), slice={[1:768:2], [0:1024:1]} | slice | bytes 3145728 | tf_op jit(solution)/shard_map/slice | solution.py:114
  199.8 7.6 %slice.280 = f32[384,1024]{1,0:T(8,128)} slice(f32[768,1024]{1,0:T(8,128)} %get-tuple-element.15), slice={[0:767:2], [0:1024:1]} | slice | bytes 3145728 | tf_op jit(solution)/shard_map/slice | solution.py:114
  207.4 5.6 fusion.66
  213.0 4.3 slice.283
  217.3 4.3 slice.284
  221.6 4.3 slice.282
  225.9 4.3 slice.286
  230.3 3.4 fusion.67
  233.6 2.7 slice.289
  236.3 2.7 slice.290
  239.0 2.7 slice.288
  241.7 2.7 slice.292
  244.4 2.4 fusion.68
  290.0 2.7 slice.287
  292.8 2.7 slice.338
  296.9 4.4 slice.281
  301.3 4.4 slice.340
  307.0 4.4 slice.342
  311.4 7.9 %slice.275 = f32[383,1024]{1,0:T(8,128)} slice(f32[768,1024]{1,0:T(8,128)} %get-tuple-element.15), slice={[2:768:2], [0:1024:1]} | slice | bytes 3137536 | tf_op jit(solution)/shard_map/slice | solution.py:114
  331.2 2.3 pad.82
  334.9 9.6 %pad.84 = f32[768,1024]{1,0:T(8,128)} pad(f32[384,1024]{1,0:T(8,128)} %add.241, f32[]{:T(128)} %constant.11.clone.1), padding=1_0_1x0_0_0 | pad | bytes 4718596 | tf_op jit(solution)/shard_map/pad | solution.py:114
  344.5 2.6 fusion.47
  347.3 5.6 pad.83
  352.9 9.5 %fusion.29 = f32[768,1024]{1,0:T(8,128)S(1)} fusion(f32[768,1024]{1,0:T(8,128)} %pad.83, f32[768,1024]{1,0:T(8,128)} %pad.84, bf16[768,2048]{0,1:T(8,128)(2,1)} %fusion.3, bf16[2048,2048]{1,0:T(8,128)(2,1)} %all-gather.5.cloned.1.call-done), kind=kOutput, calls=%fused_computation.34 | convolution fusion | flops 3230662656 | bytes 16777216 | tf_op jit(solution)/shard_map/dot_general | solution.py:68
  370.6 6.2 convolution_convert_fusion
  377.2 27.0 %all_to_all.20 = bf16[2,768,1024]{2,1,0:T(8,128)(2,1)S(1)} all-to-all(bf16[2,768,1024]{2,1,0:T(8,128)(2,1)S(1)} %bitcast.82), channel_id=1, replica_groups=mesh['rep'=2,'fs'=32,'tp'=2] {'tp'}, dimensions={0} | all-to-all | bytes 6291456 | tf_op jit(solution)/shard_map/all_to_all | solution.py:42
  407.3 2.6 copy.62
  411.5 6.3 all_to_all.21
  418.5 2.5 fusion.1
  421.0 70.5 %all-gather.9.cloned.1.call-done = bf16[2048,2816]{1,0:T(8,128)(2,1)} async-done(((bf16[64,2816]{1,0:T(8,128)(2,1)}), bf16[2048,2816]{1,0:T(8,128)(2,1)}) %all-gather.9.cloned.1.call-update) | async-done | bytes 11534352 | tf_op jit(solution)/shard_map/all_gather | solution.py:31
  491.5 9.9 %fusion.15 = f32[768,1408]{1,0:T(8,128)} fusion(bf16[768,2048]{0,1:T(8,128)(2,1)} %fusion.1, bf16[2048,2816]{1,0:T(8,128)(2,1)} %all-gather.9.cloned.1.call-done), kind=kOutput, calls=%fused_computation.25 | convolution fusion | flops 4431347712 | bytes 13238272 | tf_op jit(solution)/shard_map/dot_general | solution.py:67
  501.5 6.7 fusion.21
  508.2 143.4 %all-gather.11.cloned.1.call-done = bf16[1408,2048]{0,1:T(8,128)(2,1)} async-done(((bf16[1408,64]{0,1:T(8,128)(2,1)}), bf16[1408,2048]{0,1:T(8,128)(2,1)}) %all-gather.11.cloned.1.call-update) | async-done | bytes 5767184 | tf_op jit(solution)/shard_map/all_gather | solution.py:137
  651.7 17.5 %convolution_convert_fusion.1 = bf16[768,2048]{1,0:T(8,128)(2,1)} fusion(bf16[1408,2048]{0,1:T(8,128)(2,1)} %all-gather.11.cloned.1.call-done, f32[768,1408]{1,0:T(8,128)} %fusion.21, f32[768,1408]{1,0:T(8,128)} %fusion.15, f32[1408]{0:T(1024)S(1)} %copy-done.26, f32[1408]{0:T(1024)S(1)} %copy-done.27, f32[1408]{0:T(1024)S(1)} %copy-done.25, ...), kind=kOutput, calls=%fused_computation.28 | convolution fusion | flops 4448059392 | bytes 17597440 | tf_op jit(solution)/shard_map/dot_general | solution.py:135
  669.2 2.3 copy.85
  671.5 26.0 %all_to_all.22 = bf16[2,768,1024]{2,1,0:T(8,128)(2,1)S(1)} all-to-all(bf16[2,768,1024]{2,1,0:T(8,128)(2,1)S(1)} %bitcast.83), channel_id=1, replica_groups=mesh['rep'=2,'fs'=32,'tp'=2] {'tp'}, dimensions={0} | all-to-all | bytes 6291456 | tf_op jit(solution)/shard_map/all_to_all | solution.py:42
  (186 shorter events, 87.5 us)
Async XLA Ops:
  6.5 161.3 %copy-start = (bf16[8,128,128]{2,1,0:T(8,128)(2,1)S(1)}, bf16[8,128,128]{2,1,0:T(8,128)(2,1)}, u32[]{:S(2)}) copy-start(bf16[8,128,128]{2,1,0:T(8,128)(2,1)} %param.21) | copy-start | bytes 786436
  6.5 151.6 %all-gather.5.cloned.1.call-start = ((), (), s32[]{:S(2)}) async-start(), calls=%async_computation.4 | async-start | bytes 8650752 | tf_op jit(solution)/shard_map/all_gather | solution.py:31
  8.3 360.4 %all-gather.7.cloned.1.call-start = ((), (), s32[]{:S(2)}) async-start(), calls=%async_computation.5 | async-start | bytes 4325376 | tf_op jit(solution)/shard_map/all_gather | solution.py:122
  9.0 482.5 %all-gather.9.cloned.1.call-start = ((), (), s32[]{:S(2)}) async-start(), calls=%async_computation.6 | async-start | bytes 11894784 | tf_op jit(solution)/shard_map/all_gather | solution.py:31
  14.5 8.6 %all-to-all-start = ((bf16[2,768,1024]{1,2,0:T(8,128)(2,1)}), bf16[2,768,1024]{1,2,0:T(8,128)(2,1)S(1)}, u32[]{:S(2)}, u32[]{:S(2)}) async-start(bf16[2,768,1024]{1,2,0:T(8,128)(2,1)} %broadcast_in_dim.9), calls=%async_computation | async-start | bytes 6291456 | tf_op jit(solution)/shard_map/all_to_all | solution.py:12
  19.8 4.0 copy-start.20
  19.8 4.0 copy-start.31
  19.8 4.0 copy-start.21
  19.8 4.0 copy-start.22
  19.8 4.7 copy-start.23
  19.8 631.8 %all-gather.11.cloned.1.call-start = ((), (), s32[]{:S(2)}) async-start(), calls=%async_computation.7 | async-start | bytes 5947392 | tf_op jit(solution)/shard_map/all_gather | solution.py:137
  167.8 1.1 copy-start.9
  169.0 2.3 copy-start.33
  307.0 12.9 %copy-start.11 = (f32[3,1024]{1,0:T(4,128)S(1)}, f32[3,1024]{1,0:T(4,128)}, u32[]{:S(2)}) copy-start(f32[3,1024]{1,0:T(4,128)} %slice.320) | copy-start | bytes 36868
  307.0 12.9 %copy-start.12 = (f32[3,1024]{1,0:T(4,128)S(1)}, f32[3,1024]{1,0:T(4,128)}, u32[]{:S(2)}) copy-start(f32[3,1024]{1,0:T(4,128)} %slice.318) | copy-start | bytes 36868
  307.0 12.9 %copy-start.13 = (f32[3,1024]{1,0:T(4,128)S(1)}, f32[3,1024]{1,0:T(4,128)}, u32[]{:S(2)}) copy-start(f32[3,1024]{1,0:T(4,128)} %slice.322) | copy-start | bytes 36868
  307.0 13.0 %copy-start.14 = (f32[2,1024]{1,0:T(2,128)S(1)}, f32[2,1024]{1,0:T(2,128)}, u32[]{:S(2)}) copy-start(f32[2,1024]{1,0:T(2,128)} %slice.317) | copy-start | bytes 24580
  307.0 13.0 %copy-start.15 = (f32[2,1024]{1,0:T(2,128)S(1)}, f32[2,1024]{1,0:T(2,128)}, u32[]{:S(2)}) copy-start(f32[2,1024]{1,0:T(2,128)} %slice.328) | copy-start | bytes 24580
  307.0 15.3 %copy-start.10 = (f32[11,1024]{1,0:T(8,128)S(1)}, f32[11,1024]{1,0:T(8,128)}, u32[]{:S(2)}) copy-start(f32[11,1024]{1,0:T(8,128)} %slice.332) | copy-start | bytes 135172
  319.9 6.0 copy-start.19
  326.0 1.7 copy-start.18
  326.3 4.3 copy-start.7
  326.3 4.3 copy-start.8
  329.6 1.3 copy-start.17
  344.5 2.6 copy-start.16
  362.4 1.7 copy-start.4
  364.8 5.7 copy-start.34
  366.5 4.1 copy-start.5
  404.2 1.4 copy-start.2
  417.8 0.7 copy-start.24
  491.5 9.9 %copy-start.6 = (bf16[768,2048]{0,1:T(8,128)(2,1)S(1)}, bf16[768,2048]{0,1:T(8,128)(2,1)}, u32[]{:S(2)}) copy-start(bf16[768,2048]{0,1:T(8,128)(2,1)} %fusion.1) | copy-start | bytes 9437188
  491.5 9.9 %copy-start.32 = (bf16[2048,2816]{1,0:T(8,128)(2,1)S(1)}, bf16[2048,2816]{1,0:T(8,128)(2,1)}, u32[]{:S(2)}) copy-start(bf16[2048,2816]{1,0:T(8,128)(2,1)} %all-gather.9.cloned.1.call-done) | copy-start | bytes 34603012
  501.4 150.2 %copy-start.25 = (f32[1408]{0:T(1024)S(1)}, f32[1408]{0:T(1024)}, u32[]{:S(2)}) copy-start(f32[1408]{0:T(1024)} %get-tuple-element.8) | copy-start | bytes 16900
  501.4 150.2 %copy-start.26 = (f32[1408]{0:T(1024)S(1)}, f32[1408]{0:T(1024)}, u32[]{:S(2)}) copy-start(f32[1408]{0:T(1024)} %get-tuple-element.9) | copy-start | bytes 16900
  501.5 150.2 %copy-start.27 = (f32[1408]{0:T(1024)S(1)}, f32[1408]{0:T(1024)}, u32[]{:S(2)}) copy-start(f32[1408]{0:T(1024)} %get-tuple-element.10) | copy-start | bytes 16900
  501.5 150.2 %copy-start.28 = (f32[1408]{0:T(1024)S(1)}, f32[1408]{0:T(1024)}, u32[]{:S(2)}) copy-start(f32[1408]{0:T(1024)} %get-tuple-element.38) | copy-start | bytes 16900
  501.5 150.2 %copy-start.29 = (f32[1408]{0:T(1024)S(1)}, f32[1408]{0:T(1024)}, u32[]{:S(2)}) copy-start(f32[1408]{0:T(1024)} %get-tuple-element.39) | copy-start | bytes 16900
  501.5 150.2 %copy-start.30 = (f32[1408]{0:T(1024)S(1)}, f32[1408]{0:T(1024)}, u32[]{:S(2)}) copy-start(f32[1408]{0:T(1024)} %get-tuple-element.40) | copy-start | bytes 16900
  697.4 1.4 copy-start.3
  697.4 3.5 copy-start.1
Sparse Core Ops, SparseCore 0:
  9.0 149.0 all-gather.4
  159.7 157.1 all-gather.6
  318.6 172.8 all-gather.8
  493.0 158.5 all-gather.10
where the time goes:
time: 714 us; the launch traced here: 708 us
  waiting for transfers between devices  349 us (49%)
  local copies, waits for them, and re-layouts  161 us (23%)
  matrix products  60.1 us (8%)
  blocking collectives  59.2 us (8%)
  other arithmetic  58.8 us (8%)
  between operations  14 us (2%)
    all_gather x2, waiting for transfers between devices, side_by_side(): whole = lax.all_gather(both, axis, axis=dim, tiled=True)  202 us
    all_gather x1, waiting for transfers between devices, local(): lax.all_gather(down_weight, 'fs', axis=1, tiled=True)  143 us
    slice x56, local copies, waits for them, and re-layouts, local(): _, states = lax.associative_scan(chain_combine, (decay, driven), axis=0)  118 us
    all_to_all x2, blocking collectives, sent_and_summed(): tiles = lax.all_to_all(split_up(value, dim, count), axis, 0, 0, tiled=True)  53 us
    pad x17, local copies, waits for them, and re-layouts, local(): _, states = lax.associative_scan(chain_combine, (decay, driven), axis=0)  19.3 us
    mul x8, other arithmetic, chain_combine(): return (earlier[0] * later[0], later[0] * earlier[1] + later[1])  17.9 us
    dot_general x1, matrix products, local(): jnp.dot(hidden, lax.all_gather(down_weight, 'fs', axis=1, tiled=True), pr...  17.5 us
    dot_general x2, matrix products, pair_folder(): jnp.dot(source, pieces[0], preferred_element_type=jnp.float32)  16.6 us
  transfers between devices with their start and end apart: 5, of which 4 were waited for; matrix products, arithmetic and copies ran while one was open for 36% of the time, Pallas kernels for 0%

commit v1 on v0

--- a/solution.py
+++ b/solution.py
@@ -5,6 +5,13 @@
 
 EPS = 1e-06
 GATE_SCALE = 8.0
+
+
+def swapped_in(x, mesh_axis, dim):
+    size = lax.axis_size(mesh_axis)
+    blocks = jnp.stack([x for _ in range(size)])
+    blocks = lax.all_to_all(blocks, mesh_axis, split_axis=0, concat_axis=0)
+    return jnp.concatenate(blocks, axis=dim)
 
 
 def sent_to_all(value, axis):
@@ -133,9 +140,7 @@
     up_conv = causal_filter(up_pre.astype(jnp.float32), up_taps)
     hidden = (jax.nn.silu(gate_conv) * up_conv).astype(jnp.bfloat16)
     down_partial = jnp.dot(
-        hidden,
-        lax.all_gather(down_weight, "fs", axis=1, tiled=True),
-        preferred_element_type=jnp.float32,
+        hidden, swapped_in(down_weight, "fs", 1), preferred_element_type=jnp.float32
     )
     down_share = sent_and_summed(down_partial.astype(jnp.bfloat16), "tp", 1)
     result = (middle_own.astype(jnp.float32) + down_share).astype(jnp.bfloat16)

time: 714 us -> 638 us (0.89)
  waiting for transfers between devices: 349 us -> 250 us
  local copies, waits for them, and re-layouts: 161 us -> 174 us
    all_gather x1 -> x0, waiting for transfers between devices: 143 us -> none  [local(): lax.all_gather(down_weight, 'fs', axis=1, tiled=True)]
    all_gather x2, waiting for transfers between devices: 202 us -> 249 us  [side_by_side(): whole = lax.all_gather(both, axis, axis=dim, tiled=True)]
    slice x56, local copies, waits for them, and re-layouts: 118 us -> 130 us  [local(): _, states = lax.associative_scan(chain_combine, (decay, driven), axis=0)]
    all_to_all x1 -> x2, blocking collectives: 6.26 us -> 14.6 us  [sent_to_all(): lax.all_to_all(jnp.broadcast_to(value[None], (count, *value.shape)), axis...]
  transfers between devices with their start and end apart: 5 -> 4, of which waited for: 4 -> 2; matrix products, arithmetic and copies ran while one was open for 36% -> 42% of each run, Pallas kernels for 0% -> 0%
where the time goes in v1:
time: 638 us; the launch traced here: 625 us
  waiting for transfers between devices  250 us (39%)
  local copies, waits for them, and re-layouts  174 us (27%)
  blocking collectives  61.9 us (10%)
  other arithmetic  59.5 us (9%)
  matrix products  58.4 us (9%)
  between operations  14.1 us (2%)
  starting transfers between devices  7.52 us (1%)
    all_gather x2, waiting for transfers between devices, side_by_side(): whole = lax.all_gather(both, axis, axis=dim, tiled=True)  249 us
    slice x56, local copies, waits for them, and re-layouts, local(): _, states = lax.associative_scan(chain_combine, (decay, driven), axis=0)  130 us
    all_to_all x2, blocking collectives, sent_and_summed(): tiles = lax.all_to_all(split_up(value, dim, count), axis, 0, 0, tiled=True)  47.2 us
    pad x17, local copies, waits for them, and re-layouts, local(): _, states = lax.associative_scan(chain_combine, (decay, driven), axis=0)  19.5 us
    mul x8, other arithmetic, chain_combine(): return (earlier[0] * later[0], later[0] * earlier[1] + later[1])  17.9 us
    dot_general x1, matrix products, local(): jnp.dot(hidden, swapped_in(down_weight, 'fs', 1), preferred_element_type=...  17.5 us
    dot_general x2, matrix products, pair_folder(): jnp.dot(source, pieces[1], preferred_element_type=jnp.float32)  16.2 us
    dot_general x2, matrix products, pair_folder(): jnp.dot(source, pieces[0], preferred_element_type=jnp.float32)  15.1 us
  transfers between devices with their start and end apart: 4, of which 2 were waited for; matrix products, arithmetic and copies ran while one was open for 42% of the time, Pallas kernels for 0%

profile of v1, /device:TPU:1, one launch (start us, length us, event | category | flops | bytes accessed | tf_op | source)
XLA Modules:
  0.0 625.5 jit_solution(1235947694335623603)
XLA Ops:
  12.8 7.3 %all_to_all.25 = bf16[2,768,1024]{1,2,0:T(8,128)(2,1)S(1)} all-to-all(bf16[2,768,1024]{1,2,0:T(8,128)(2,1)S(1)} %broadcast_in_dim.9), channel_id=1, replica_groups=mesh['rep'=2,'fs'=32,'tp'=2] {'tp'}, dimensions={0} | all-to-all | bytes 6291456 | tf_op jit(solution)/shard_map/all_to_all | solution.py:19
  21.7 136.4 %all-gather.4.cloned.1.call-done = bf16[2048,2048]{1,0:T(8,128)(2,1)} async-done(((bf16[64,2048]{1,0:T(8,128)(2,1)}), bf16[2048,2048]{1,0:T(8,128)(2,1)}) %all-gather.4.cloned.1.call-update) | async-done | bytes 8388624 | tf_op jit(solution)/shard_map/all_gather | solution.py:38
  158.1 5.2 fusion.38
  163.4 3.1 convert_bitcast_fusion
  167.6 2.4 copy.67
  170.0 2.5 add_divide_fusion
  172.5 2.4 copy.68
  174.9 7.7 %multiply_exponential_fusion = (f32[768,1024]{1,0:T(8,128)}, f32[768,1024]{1,0:T(8,128)S(1)}) fusion(f32[768,1024]{1,0:T(8,128)} %copy.67, f32[1024]{0:T(1024)S(1)} %fusion.62, f32[768,1024]{1,0:T(8,128)} %get-tuple-element.14, f32[768,1024]{1,0:T(8,128)} %copy.68), kind=kLoop, calls=%fused_computation.51 | loop fusion | flops 3932160 | bytes 15732736 | tf_op jit(solution)/shard_map/exp | solution.py:119
  182.6 4.2 slice.277
  186.8 4.2 slice.278
  191.0 7.6 %slice.276 = f32[384,1024]{1,0:T(8,128)} slice(f32[768,1024]{1,0:T(8,128)} %get-tuple-element.15), slice={[1:768:2], [0:1024:1]} | slice | bytes 3145728 | tf_op jit(solution)/shard_map/slice | solution.py:121
  198.6 7.6 %slice.280 = f32[384,1024]{1,0:T(8,128)} slice(f32[768,1024]{1,0:T(8,128)} %get-tuple-element.15), slice={[0:767:2], [0:1024:1]} | slice | bytes 3145728 | tf_op jit(solution)/shard_map/slice | solution.py:121
  206.2 5.5 fusion.66
  211.7 4.3 slice.283
  216.0 4.3 slice.284
  220.4 4.3 slice.282
  224.7 4.3 slice.286
  229.0 3.4 fusion.67
  232.4 2.7 slice.289
  235.1 2.7 slice.290
  237.8 2.7 slice.288
  240.5 2.7 slice.292
  243.2 2.4 fusion.68
  250.6 13.2 %slice.298 = f32[48,1024]{1,0:T(8,128)} slice(f32[96,1024]{1,0:T(8,128)} %get-tuple-element.21), slice={[0:95:2], [0:1024:1]} | slice | bytes 393216 | tf_op jit(solution)/shard_map/slice | solution.py:121
  300.5 2.8 slice.287
  303.3 2.8 slice.338
  307.4 4.4 slice.340
  311.8 4.4 slice.281
  317.5 4.4 slice.342
  321.9 7.7 %slice.275 = f32[383,1024]{1,0:T(8,128)} slice(f32[768,1024]{1,0:T(8,128)} %get-tuple-element.15), slice={[2:768:2], [0:1024:1]} | slice | bytes 3137536 | tf_op jit(solution)/shard_map/slice | solution.py:121
  341.5 2.3 pad.82
  345.2 9.8 %pad.84 = f32[768,1024]{1,0:T(8,128)} pad(f32[384,1024]{1,0:T(8,128)} %add.241, f32[]{:T(128)} %constant.11.clone.1), padding=1_0_1x0_0_0 | pad | bytes 4718596 | tf_op jit(solution)/shard_map/pad | solution.py:121
  355.0 2.6 fusion.47
  357.7 5.7 pad.83
  363.4 9.5 %fusion.29 = f32[768,1024]{1,0:T(8,128)S(1)} fusion(f32[768,1024]{1,0:T(8,128)} %pad.83, f32[768,1024]{1,0:T(8,128)} %pad.84, bf16[768,2048]{0,1:T(8,128)(2,1)} %copy-done.7, bf16[2048,2048]{1,0:T(8,128)(2,1)} %all-gather.4.cloned.1.call-done), kind=kOutput, calls=%fused_computation.34 | convolution fusion | flops 3230662656 | bytes 16777216 | tf_op jit(solution)/shard_map/dot_general | solution.py:75
  381.1 6.0 convolution_convert_fusion
  387.5 26.9 %all_to_all.26 = bf16[2,768,1024]{2,1,0:T(8,128)(2,1)S(1)} all-to-all(bf16[2,768,1024]{2,1,0:T(8,128)(2,1)S(1)} %bitcast.85), channel_id=1, replica_groups=mesh['rep'=2,'fs'=32,'tp'=2] {'tp'}, dimensions={0} | all-to-all | bytes 6291456 | tf_op jit(solution)/shard_map/all_to_all | solution.py:49
  417.5 2.7 copy.63
  421.8 7.4 %all_to_all.27 = bf16[2,768,1024]{1,2,0:T(8,128)(2,1)} all-to-all(bf16[2,768,1024]{1,2,0:T(8,128)(2,1)S(1)} %broadcast_in_dim.11), channel_id=1, replica_groups=mesh['rep'=2,'fs'=32,'tp'=2] {'tp'}, dimensions={0} | all-to-all | bytes 6291456 | tf_op jit(solution)/shard_map/all_to_all | solution.py:19
  429.2 3.2 stack.2
  432.4 7.4 %all-to-all-start.3 = ((bf16[32,1408,64]{1,2,0:T(8,128)(2,1)}), bf16[32,1408,64]{1,2,0:T(8,128)(2,1)}, u32[]{:S(2)}, u32[]{:S(2)}) async-start(bf16[32,1408,64]{1,2,0:T(8,128)(2,1)} %stack.2), calls=%async_computation.3 | async-start | bytes 11534336 | tf_op jit(solution)/shard_map/all_to_all | solution.py:13
  440.0 2.8 multiply_reduce_fusion
  442.8 2.5 fusion.1
  445.3 113.0 %all-gather.8.cloned.1.call-done = bf16[2048,2816]{1,0:T(8,128)(2,1)} async-done(((bf16[64,2816]{1,0:T(8,128)(2,1)}), bf16[2048,2816]{1,0:T(8,128)(2,1)}) %all-gather.8.cloned.1.call-update) | async-done | bytes 11534352 | tf_op jit(solution)/shard_map/all_gather | solution.py:38
  558.4 9.9 %fusion.15 = f32[768,1408]{1,0:T(8,128)} fusion(bf16[768,2048]{0,1:T(8,128)(2,1)} %fusion.1, bf16[2048,2816]{1,0:T(8,128)(2,1)} %all-gather.8.cloned.1.call-done), kind=kOutput, calls=%fused_computation.25 | convolution fusion | flops 4431347712 | bytes 13238272 | tf_op jit(solution)/shard_map/dot_general | solution.py:74
  568.3 6.7 %fusion.21 = f32[768,1408]{1,0:T(8,128)} fusion(bf16[768,2048]{0,1:T(8,128)(2,1)S(1)} %copy-done.8, bf16[2048,2816]{1,0:T(8,128)(2,1)S(1)} %copy-done.29), kind=kOutput, calls=%fused_computation.27 | convolution fusion | flops 4431347712 | bytes 13238272 | tf_op jit(solution)/shard_map/dot_general | solution.py:75
  574.9 17.5 %convolution_convert_fusion.1 = bf16[768,2048]{1,0:T(8,128)(2,1)} fusion(bf16[1408,2048]{0,1:T(8,128)(2,1)} %bitcast.17, f32[768,1408]{1,0:T(8,128)} %fusion.21, f32[768,1408]{1,0:T(8,128)} %fusion.15, f32[1408]{0:T(1024)S(1)} %get-tuple-element.9, f32[1408]{0:T(1024)S(1)} %get-tuple-element.10, f32[1408]{0:T(1024)S(1)} %get-tuple-element.8, ...), kind=kOutput, calls=%fused_computation.28 | convolution fusion | flops 4448059392 | bytes 17597440 | tf_op jit(solution)/shard_map/dot_general | solution.py:142
  594.7 20.3 %all_to_all.28 = bf16[2,768,1024]{2,1,0:T(8,128)(2,1)S(1)} all-to-all(bf16[2,768,1024]{2,1,0:T(8,128)(2,1)S(1)} %bitcast.86), channel_id=1, replica_groups=mesh['rep'=2,'fs'=32,'tp'=2] {'tp'}, dimensions={0} | all-to-all | bytes 6291456 | tf_op jit(solution)/shard_map/all_to_all | solution.py:49
  (179 shorter events, 85.5 us)
Async XLA Ops:
  6.5 159.9 %copy-start = (bf16[8,128,128]{2,1,0:T(8,128)(2,1)S(1)}, bf16[8,128,128]{2,1,0:T(8,128)(2,1)}, u32[]{:S(2)}) copy-start(bf16[8,128,128]{2,1,0:T(8,128)(2,1)} %param.21) | copy-start | bytes 786436
  6.5 151.5 %all-gather.4.cloned.1.call-start = ((), (), s32[]{:S(2)}) async-start(), calls=%async_computation.5 | async-start | bytes 8650752 | tf_op jit(solution)/shard_map/all_gather | solution.py:38
  8.3 370.9 %all-gather.6.cloned.1.call-start = ((), (), s32[]{:S(2)}) async-start(), calls=%async_computation.6 | async-start | bytes 4325376 | tf_op jit(solution)/shard_map/all_gather | solution.py:129
  9.0 549.3 %all-gather.8.cloned.1.call-start = ((), (), s32[]{:S(2)}) async-start(), calls=%async_computation.7 | async-start | bytes 11894784 | tf_op jit(solution)/shard_map/all_gather | solution.py:38
  20.1 0.7 copy-start.28
  20.1 0.7 copy-start.23
  20.1 0.8 copy-start.26
  21.7 141.7 %copy-start.7 = (bf16[768,2048]{0,1:T(8,128)(2,1)}, bf16[768,2048]{0,1:T(8,128)(2,1)S(1)}, u32[]{:S(2)}) copy-start(bf16[768,2048]{0,1:T(8,128)(2,1)S(1)} %fusion.3) | copy-start | bytes 9437188
  166.4 1.1 copy-start.11
  167.6 2.4 copy-start.30
  317.5 12.7 %copy-start.14 = (f32[3,1024]{1,0:T(4,128)S(1)}, f32[3,1024]{1,0:T(4,128)}, u32[]{:S(2)}) copy-start(f32[3,1024]{1,0:T(4,128)} %slice.320) | copy-start | bytes 36868
  317.5 12.7 %copy-start.15 = (f32[3,1024]{1,0:T(4,128)S(1)}, f32[3,1024]{1,0:T(4,128)}, u32[]{:S(2)}) copy-start(f32[3,1024]{1,0:T(4,128)} %slice.318) | copy-start | bytes 36868
  317.5 12.7 %copy-start.16 = (f32[3,1024]{1,0:T(4,128)S(1)}, f32[3,1024]{1,0:T(4,128)}, u32[]{:S(2)}) copy-start(f32[3,1024]{1,0:T(4,128)} %slice.322) | copy-start | bytes 36868
  317.5 12.8 %copy-start.17 = (f32[2,1024]{1,0:T(2,128)S(1)}, f32[2,1024]{1,0:T(2,128)}, u32[]{:S(2)}) copy-start(f32[2,1024]{1,0:T(2,128)} %slice.317) | copy-start | bytes 24580
  317.5 12.8 %copy-start.18 = (f32[2,1024]{1,0:T(2,128)S(1)}, f32[2,1024]{1,0:T(2,128)}, u32[]{:S(2)}) copy-start(f32[2,1024]{1,0:T(2,128)} %slice.328) | copy-start | bytes 24580
  317.5 15.1 %copy-start.12 = (f32[11,1024]{1,0:T(8,128)S(1)}, f32[11,1024]{1,0:T(8,128)}, u32[]{:S(2)}) copy-start(f32[11,1024]{1,0:T(8,128)} %slice.332) | copy-start | bytes 135172
  330.2 6.0 copy-start.22
  336.2 1.7 copy-start.21
  336.6 4.3 copy-start.9
  336.6 4.3 copy-start.10
  339.9 1.3 copy-start.20
  354.9 2.6 copy-start.19
  372.9 1.7 copy-start.5
  375.3 5.7 copy-start.31
  376.9 4.1 copy-start.6
  414.4 1.4 copy-start.3
  421.8 7.4 %copy-start.13 = (bf16[1408,64]{0,1:T(8,128)(2,1)S(1)}, bf16[1408,64]{0,1:T(8,128)(2,1)}, u32[]{:S(2)}) copy-start(bf16[1408,64]{0,1:T(8,128)(2,1)} %param.31) | copy-start | bytes 540676
  432.4 7.5 %copy-start.24 = (f32[3,1408]{1,0:T(4,128)S(1)}, f32[3,1408]{1,0:T(4,128)}, u32[]{:S(2)}) copy-start(f32[3,1408]{1,0:T(4,128)} %param.30) | copy-start | bytes 50692
  432.4 7.5 %copy-start.25 = (f32[3,1408]{1,0:T(4,128)S(1)}, f32[3,1408]{1,0:T(4,128)}, u32[]{:S(2)}) copy-start(f32[3,1408]{1,0:T(4,128)} %param.29) | copy-start | bytes 50692
  432.4 142.5 %all-to-all-start.3 = ((bf16[32,1408,64]{1,2,0:T(8,128)(2,1)}), bf16[32,1408,64]{1,2,0:T(8,128)(2,1)}, u32[]{:S(2)}, u32[]{:S(2)}) async-start(bf16[32,1408,64]{1,2,0:T(8,128)(2,1)} %stack.2), calls=%async_computation.3 | async-start | bytes 11534336 | tf_op jit(solution)/shard_map/all_to_all | solution.py:13
  439.9 2.9 copy-start.2
  439.9 2.9 copy-start.27
  558.4 9.9 %copy-start.8 = (bf16[768,2048]{0,1:T(8,128)(2,1)S(1)}, bf16[768,2048]{0,1:T(8,128)(2,1)}, u32[]{:S(2)}) copy-start(bf16[768,2048]{0,1:T(8,128)(2,1)} %fusion.1) | copy-start | bytes 9437188
  558.4 9.9 %copy-start.29 = (bf16[2048,2816]{1,0:T(8,128)(2,1)S(1)}, bf16[2048,2816]{1,0:T(8,128)(2,1)}, u32[]{:S(2)}) copy-start(bf16[2048,2816]{1,0:T(8,128)(2,1)} %all-gather.8.cloned.1.call-done) | copy-start | bytes 34603012
  615.1 1.4 copy-start.4
  615.1 3.5 copy-start.1
Sparse Core Ops, SparseCore 0:
  9.0 149.0 all-gather.3
  159.7 157.1 all-gather.5
  318.6 239.7 all-gather.7
